TPU v7x, 32 devices: a whole 2x2x4 slice. The times are simulated.
32 devices in a mesh: sp: 8 (over z, y), tp: 4 (over x, core).
Axes of the slice: x: 2, y: 2, z: 4, core: 2. Of those that a mesh axis runs over, the one named last changes fastest.
Arguments:
- tokens: bfloat16 [6144, 4096], P('sp', 'tp'), may hold values from -6 to 6
- in_proj: bfloat16 [3, 4096, 1024], P(None, 'tp', 'sp'), may hold values from -0.09375 to 0.09375
- group_mix: bfloat16 [3, 4, 256, 256], replicated, may hold values from -0.375 to 0.375
- pool_gain: float32 [3, 1024], replicated, may hold values from 0.1 to 1.9
- out_proj: bfloat16 [3, 1024, 4096], P(None, 'sp', 'tp'), may hold values from -0.1875 to 0.1875
- norm_gain: float32 [3, 4096], P(None, 'tp'), may hold values from 0.25 to 3
- norm_bias: float32 [3, 4096], P(None, 'tp'), may hold values from -1.5 to 1.5
Outputs:
- stream_out: bfloat16 [6144, 4096], P('sp', 'tp')
All inputs are finite; a program needn't handle non-finite values.
Results may differ from a plain program's by a relative error of at most 0.017.
Values may be sent and summed in bfloat16 or wider, within the bound.
A program may use at most 128 MiB of HBM per device.

v0:
```python
import jax
import jax.numpy as jnp
from jax import lax
from jax.sharding import PartitionSpec as P

pool_windows = (2, 4, 8, 16)
norm_eps = 1e-05


def padded(array, sides, width):
    for axis, dim in sides:
        devices, length = (lax.axis_size(axis), array.shape[dim])
        up = [(i, (i + 1) % devices) for i in range(devices - 1)]
        down = [(j, i) for i, j in up]
        last = lax.slice_in_dim(array, length - width, length, axis=dim)
        leading = lax.slice_in_dim(array, 0, width, axis=dim)
        before = lax.ppermute(last, axis, up)
        after = lax.ppermute(leading, axis, down)
        array = jnp.concatenate([before, array, after], axis=dim)
    return array


def on_device(tokens, in_proj, group_mix, pool_gain, out_proj, norm_gain, norm_bias):
    rows_dev = tokens.shape[0]
    feat_dev = tokens.shape[1]
    layer_count = in_proj.shape[0]
    pool_width = in_proj.shape[2] * lax.axis_size("sp")
    chan_share = pool_width // lax.axis_size("tp")
    group_width = group_mix.shape[2]
    model_width = feat_dev * lax.axis_size("tp")
    residual_scale = (2.0 * layer_count) ** 0.25
    fringe_width = max(pool_windows) // 2
    seq_length = rows_dev * lax.axis_size("sp")
    positions = lax.axis_index("sp") * rows_dev + jnp.arange(rows_dev)
    chan_groups = (lax.axis_index("tp") * chan_share + jnp.arange(chan_share)) // group_width
    in_all, out_all = (
        lax.all_gather(in_proj, "sp", axis=2, tiled=True),
        lax.all_gather(out_proj, "sp", axis=1, tiled=True),
    )
    stream = tokens
    for layer_idx in range(layer_count):
        in_block = in_all[layer_idx]
        out_block = out_all[layer_idx]
        projected = lax.psum_scatter(
            lax.dot_general(
                in_block, stream, (((0,), (1,)), ((), ())), preferred_element_type=jnp.float32
            ).astype(jnp.bfloat16),
            "tp",
            scatter_dimension=0,
            tiled=True,
        )
        extended = padded(projected, (("sp", 1),), fringe_width)
        ext_float = extended.astype(jnp.float32)
        pooled = jnp.zeros((chan_share, rows_dev), jnp.float32)
        for group_idx in range(4):
            own_rows = (chan_groups == group_idx)[:, None]
            span_len = pool_windows[group_idx]
            before = span_len // 2
            after = span_len - before
            window_total = jnp.zeros((ext_float.shape[0], rows_dev), jnp.float32)
            for offset in range(-before, after):
                window_total = (
                    window_total
                    + ext_float[:, fringe_width + offset : fringe_width + offset + rows_dev]
                )
            low_edge = jnp.clip(positions - before, 0, seq_length)
            high_edge = jnp.clip(positions + after, 0, seq_length)
            pooled = jnp.where(
                own_rows, window_total / (high_edge - low_edge).astype(jnp.float32)[None, :], pooled
            )
        differ = (pooled - projected.astype(jnp.float32)).astype(jnp.bfloat16)
        all_differ = lax.all_gather(differ, "tp", axis=0, tiled=True)
        grouped = all_differ.reshape(4, group_width, rows_dev)
        mixed_all = jnp.einsum(
            "gcd,gct->gdt", group_mix[layer_idx], grouped, preferred_element_type=jnp.float32
        ).reshape(pool_width, rows_dev)
        mixed_all = (mixed_all * pool_gain[layer_idx][:, None]).astype(jnp.bfloat16)
        branch = lax.dot_general(
            mixed_all, out_block, (((0,), (0,)), ((), ())), preferred_element_type=jnp.float32
        )
        resid = residual_scale * stream.astype(jnp.float32) + branch
        row_sums, squares = lax.psum((jnp.sum(resid, axis=1), jnp.sum(resid * resid, axis=1)), "tp")
        row_mean = row_sums / model_width
        row_var = squares / model_width - row_mean * row_mean
        normed = (resid - row_mean[:, None]) * lax.rsqrt(row_var[:, None] + norm_eps)
        stream = (normed * norm_gain[layer_idx][None, :] + norm_bias[layer_idx][None, :]).astype(
            jnp.bfloat16
        )
    return stream


def solution(mesh):
    in_specs = (
        P("sp", "tp"),
        P(None, "tp", "sp"),
        P(),
        P(),
        P(None, "sp", "tp"),
        P(None, "tp"),
        P(None, "tp"),
    )
    out_specs = P("sp", "tp")
    return jax.shard_map(
        on_device, mesh=mesh, in_specs=in_specs, out_specs=out_specs, check_vma=False
    )
```

profile of v0, /device:TPU:0, one launch (start us, length us, event | category | flops | bytes accessed | tf_op | source)
XLA Modules:
  0.0 468.3 jit_solution(7111326799867742258)
XLA Ops:
  6.5 0.7 all-gather.6.cloned.1.call-update
  7.3 104.3 %all-gather.6.cloned.1.call-done = bf16[3,1024,1024]{2,1,0:T(8,128)(2,1)} async-done(((bf16[3,1024,128]{2,1,0:T(8,128)(2,1)}), bf16[3,1024,1024]{2,1,0:T(8,128)(2,1)}) %all-gather.6.cloned.1.call-update) | async-done | bytes 6291472 | tf_op jit(solution)/shard_map/all_gather | solution.py:37
  111.6 5.0 %fusion.6 = bf16[1024,768]{1,0:T(8,128)(2,1)} fusion(bf16[768,1024]{1,0:T(8,128)(2,1)} %param.7, bf16[3,1024,1024]{2,1,0:T(8,128)(2,1)} %all-gather.6.cloned.1.call-done), kind=kOutput, calls=%fused_computation.24 | convolution fusion | flops 1611399168 | bytes 5242880 | tf_op jit(solution)/shard_map/dot_general | solution.py:45
  116.7 0.0 all-gather.8.cloned.1.call-start
  116.8 26.3 %reduce-scatter.4.cloned.1.call-done = bf16[256,768]{1,0:T(8,128)(2,1)} async-done(((bf16[1024,768]{1,0:T(8,128)(2,1)}), bf16[256,768]{1,0:T(8,128)(2,1)}) %reduce-scatter.4.cloned.1.call-update) | async-done | bytes 393232 | tf_op jit(solution)/shard_map/reduce_scatter | solution.py:44
  143.0 1.0 fusion.58
  144.0 3.4 collective-permute-start
  147.4 1.3 collective-permute-start.1
  148.7 0.6 collective-permute-done
  149.3 4.3 collective-permute-done.1
  153.6 1.2 maximum_convert_fusion
  154.8 5.1 %fusion.44 = bf16[256,768]{1,0:T(8,128)(2,1)} fusion(bf16[256,768]{1,0:T(8,128)(2,1)} %reduce-scatter.4.cloned.1.call-done, f32[256,784]{1,0:T(8,128)S(1)} %maximum_convert_fusion, f32[768]{0:T(1024)S(1)} %get-tuple-element.41, f32[768]{0:T(1024)S(1)} %get-tuple-element.42, f32[768]{0:T(1024)S(1)} %get-tuple-element.43, f32[768]{0:T(1024)S(1)} %get-tuple-element.44, ...), kind=kLoop, calls=%fused_computation.83 | loop fusion | flops 7274496 | bytes 13382656 | tf_op jit(solution)/shard_map/convert_element_type | solution.py:71
  160.0 0.5 all-gather.10.cloned.1.call-update
  160.7 19.0 %all-gather.8.cloned.1.call-done = bf16[1024,768]{1,0:T(8,128)(2,1)} async-done(((bf16[256,768]{1,0:T(8,128)(2,1)}), bf16[1024,768]{1,0:T(8,128)(2,1)}) %all-gather.8.cloned.1.call-update) | async-done | bytes 1572880 | tf_op jit(solution)/shard_map/all_gather | solution.py:72
  179.7 2.0 multiply_convert_fusion.2
  181.7 98.7 %all-gather.10.cloned.1.call-done = bf16[3,1024,1024]{2,1,0:T(8,128)(2,1)} async-done(((bf16[3,128,1024]{2,1,0:T(8,128)(2,1)}), bf16[3,1024,1024]{2,1,0:T(8,128)(2,1)}) %all-gather.10.cloned.1.call-update) | async-done | bytes 6291472 | tf_op jit(solution)/shard_map/all_gather | solution.py:38
  280.5 5.8 %fusion.55 = (f32[768]{0:T(1024)S(1)}, f32[768]{0:T(1024)S(1)}, f32[768,1024]{1,0:T(8,128)}) fusion(bf16[1024,768]{1,0:T(8,128)(2,1)S(1)} %bitcast.86, bf16[3,1024,1024]{2,1,0:T(8,128)(2,1)} %all-gather.10.cloned.1.call-done, bf16[768,1024]{1,0:T(8,128)(2,1)} %param.7), kind=kOutput, calls=%fused_computation.119 | convolution fusion | flops 1615329792 | bytes 8394752 | tf_op jit(solution)/shard_map/dot_general | solution.py:78
  286.2 5.7 %all-reduce.2 = (f32[768]{0:T(1024)S(1)}, f32[768]{0:T(1024)S(1)}) all-reduce(f32[768]{0:T(1024)S(1)} %get-tuple-element.10, f32[768]{0:T(1024)S(1)} %get-tuple-element.9), channel_id=1, replica_groups=mesh['sp'=8,'tp'=4] {'tp'}, use_global_device_ids=true, to_apply=%region_4.5 | all-reduce | flops 1536 | bytes 12288 | tf_op jit(solution)/shard_map/psum | solution.py:82
  292.0 5.9 %fusion.10 = bf16[1024,768]{1,0:T(8,128)(2,1)} fusion(bf16[3,1024,1024]{2,1,0:T(8,128)(2,1)} %all-gather.6.cloned.1.call-done, f32[768,1024]{1,0:T(8,128)} %get-tuple-element.38, f32[1024]{0:T(1024)S(1)} %bitcast.95, f32[1024]{0:T(1024)S(1)} %bitcast.93, f32[768]{0:T(1024)S(1)} %get-tuple-element.37, f32[768]{0:T(1024)S(1)} %get-tuple-element.36), kind=kOutput, calls=%fused_computation.28 | convolution fusion | flops 1615331328 | bytes 6830080 | tf_op jit(solution)/shard_map/dot_general | solution.py:45
  298.0 26.6 %reduce-scatter.6.cloned.1.call-done = bf16[256,768]{1,0:T(8,128)(2,1)} async-done(((bf16[1024,768]{1,0:T(8,128)(2,1)}), bf16[256,768]{1,0:T(8,128)(2,1)}) %reduce-scatter.6.cloned.1.call-update) | async-done | bytes 393232 | tf_op jit(solution)/shard_map/reduce_scatter | solution.py:44
  324.6 1.0 fusion.57
  325.6 3.4 collective-permute-start.2
  328.9 1.3 collective-permute-start.3
  330.2 0.6 collective-permute-done.2
  330.8 4.3 collective-permute-done.3
  335.1 1.2 maximum_convert_fusion.1
  336.3 5.0 %fusion.45 = bf16[256,768]{1,0:T(8,128)(2,1)} fusion(bf16[256,768]{1,0:T(8,128)(2,1)} %reduce-scatter.6.cloned.1.call-done, f32[256,784]{1,0:T(8,128)S(1)} %maximum_convert_fusion.1, f32[768]{0:T(1024)S(1)} %get-tuple-element.41, f32[768]{0:T(1024)S(1)} %get-tuple-element.42, f32[768]{0:T(1024)S(1)} %get-tuple-element.43, f32[768]{0:T(1024)S(1)} %get-tuple-element.44, ...), kind=kLoop, calls=%fused_computation.84 | loop fusion | flops 7274496 | bytes 13382656 | tf_op jit(solution)/shard_map/convert_element_type | solution.py:71
  341.3 0.2 reduce-scatter.8.cloned.1.call-start
  341.5 19.5 %all-gather.12.cloned.1.call-done = bf16[1024,768]{1,0:T(8,128)(2,1)} async-done(((bf16[256,768]{1,0:T(8,128)(2,1)}), bf16[1024,768]{1,0:T(8,128)(2,1)}) %all-gather.12.cloned.1.call-update) | async-done | bytes 1572880 | tf_op jit(solution)/shard_map/all_gather | solution.py:72
  361.1 2.2 multiply_convert_fusion.1
  363.3 0.2 copy-done.4
  363.5 5.9 %fusion.54 = (f32[768]{0:T(1024)S(1)}, f32[768]{0:T(1024)S(1)}, f32[768,1024]{1,0:T(8,128)}) fusion(bf16[1024,768]{1,0:T(8,128)(2,1)S(1)} %bitcast.85, bf16[3,1024,1024]{2,1,0:T(8,128)(2,1)} %all-gather.10.cloned.1.call-done, f32[1024]{0:T(1024)S(1)} %bitcast.96, f32[1024]{0:T(1024)S(1)} %bitcast.94, f32[768]{0:T(1024)S(1)} %get-tuple-element.37, ...), kind=kOutput, calls=%fused_computation.118 | convolution fusion | flops 1619261952 | bytes 9981952 | tf_op jit(solution)/shard_map/dot_general | solution.py:78
  369.3 6.0 %all-reduce.1 = (f32[768]{0:T(1024)S(1)}, f32[768]{0:T(1024)S(1)}) all-reduce(f32[768]{0:T(1024)S(1)} %get-tuple-element.8, f32[768]{0:T(1024)S(1)} %get-tuple-element.7), channel_id=1, replica_groups=mesh['sp'=8,'tp'=4] {'tp'}, use_global_device_ids=true, to_apply=%region_9.10 | all-reduce | flops 1536 | bytes 12288 | tf_op jit(solution)/shard_map/psum | solution.py:82
  375.3 5.9 %fusion.9 = bf16[1024,768]{1,0:T(8,128)(2,1)} fusion(bf16[3,1024,1024]{2,1,0:T(8,128)(2,1)} %all-gather.6.cloned.1.call-done, f32[768,1024]{1,0:T(8,128)} %get-tuple-element.39, f32[1024]{0:T(1024)S(1)} %bitcast.91, f32[1024]{0:T(1024)S(1)} %bitcast.89, f32[768]{0:T(1024)S(1)} %get-tuple-element.35, f32[768]{0:T(1024)S(1)} %get-tuple-element.34), kind=kOutput, calls=%fused_computation.27 | convolution fusion | flops 1615331328 | bytes 6830080 | tf_op jit(solution)/shard_map/dot_general | solution.py:45
  381.3 29.2 %reduce-scatter.8.cloned.1.call-done = bf16[256,768]{1,0:T(8,128)(2,1)} async-done(((bf16[1024,768]{1,0:T(8,128)(2,1)}), bf16[256,768]{1,0:T(8,128)(2,1)}) %reduce-scatter.8.cloned.1.call-update) | async-done | bytes 393232 | tf_op jit(solution)/shard_map/reduce_scatter | solution.py:44
  410.5 1.0 fusion.56
  411.5 3.4 collective-permute-start.4
  414.8 1.3 collective-permute-start.5
  416.1 0.6 collective-permute-done.4
  416.7 4.3 collective-permute-done.5
  421.0 1.2 maximum_convert_fusion.2
  422.2 5.0 %fusion.46 = bf16[256,768]{1,0:T(8,128)(2,1)} fusion(bf16[256,768]{1,0:T(8,128)(2,1)} %reduce-scatter.8.cloned.1.call-done, f32[256,784]{1,0:T(8,128)S(1)} %maximum_convert_fusion.2, f32[768]{0:T(1024)S(1)} %get-tuple-element.41, f32[768]{0:T(1024)S(1)} %get-tuple-element.42, f32[768]{0:T(1024)S(1)} %get-tuple-element.43, f32[768]{0:T(1024)S(1)} %get-tuple-element.44, ...), kind=kLoop, calls=%fused_computation.85 | loop fusion | flops 7274496 | bytes 13382656 | tf_op jit(solution)/shard_map/convert_element_type | solution.py:71
  427.2 19.8 %all-gather.14.cloned.1.call-done = bf16[1024,768]{1,0:T(8,128)(2,1)} async-done(((bf16[256,768]{1,0:T(8,128)(2,1)}), bf16[1024,768]{1,0:T(8,128)(2,1)}) %all-gather.14.cloned.1.call-update) | async-done | bytes 1572880 | tf_op jit(solution)/shard_map/all_gather | solution.py:72
  447.0 2.2 multiply_convert_fusion
  449.2 0.2 copy-done.5
  449.4 4.4 fusion.53
  453.7 6.0 %all-reduce = (f32[768]{0:T(1024)S(1)}, f32[768]{0:T(1024)S(1)}) all-reduce(f32[768]{0:T(1024)S(1)} %get-tuple-element.6, f32[768]{0:T(1024)S(1)} %get-tuple-element.5), channel_id=1, replica_groups=mesh['sp'=8,'tp'=4] {'tp'}, use_global_device_ids=true, to_apply=%region_14.15 | all-reduce | flops 1536 | bytes 12288 | tf_op jit(solution)/shard_map/psum | solution.py:82
  459.7 1.7 add_convert_fusion
  (35 shorter events, 0.5 us)
Async XLA Ops:
  6.5 105.1 %all-gather.6.cloned.1.call-start = ((), (), s32[]{:S(2)}) async-start(), calls=%async_computation.3 | async-start | bytes 7077888 | tf_op jit(solution)/shard_map/all_gather | solution.py:37
  7.3 135.8 %reduce-scatter.4.cloned.1.call-start = ((), (), s32[]{:S(2)}) async-start(), calls=%async_computation.4 | async-start | bytes 1966080 | tf_op jit(solution)/shard_map/reduce_scatter | solution.py:44
  116.7 63.0 %all-gather.8.cloned.1.call-start = ((), (), s32[]{:S(2)}) async-start(), calls=%async_computation.5 | async-start | bytes 1966080 | tf_op jit(solution)/shard_map/all_gather | solution.py:72
  144.0 5.3 %collective-permute-start = (bf16[256,8]{1,0:T(8,128)(2,1)S(1)}, bf16[256,8]{1,0:T(8,128)(2,1)S(1)}, u32[]{:S(2)}, u32[]{:S(2)}) collective-permute-start(bf16[256,8]{1,0:T(8,128)(2,1)S(1)} %get-tuple-element.24), channel_id=1, source_target_pairs={{0,4},{4,8},{8,12},{12,16},{16,20},{20,24},{24,28},{1,5},{5,9},{9,... | collective-permute-start | bytes 12296 | tf_op jit(solution)/shard_map/ppermute | solution.py:17
  147.4 6.2 %collective-permute-start.1 = (bf16[256,8]{1,0:T(8,128)(2,1)S(1)}, bf16[256,8]{1,0:T(8,128)(2,1)S(1)}, u32[]{:S(2)}, u32[]{:S(2)}) collective-permute-start(bf16[256,8]{1,0:T(8,128)(2,1)S(1)} %get-tuple-element.25), channel_id=1, source_target_pairs={{4,0},{8,4},{12,8},{16,12},{20,16},{24,20},{28,24},{5,1},{9,5},{13... | collective-permute-start | bytes 12296 | tf_op jit(solution)/shard_map/ppermute | solution.py:18
  154.8 5.8 %copy-start.1 = (f32[3,1024]{1,0:T(4,128)S(1)}, f32[3,1024]{1,0:T(4,128)}, u32[]{:S(2)}) copy-start(f32[3,1024]{1,0:T(4,128)} %param.10) | copy-start | bytes 36868
  154.8 5.8 %copy-start.2 = (f32[3,1024]{1,0:T(4,128)S(1)}, f32[3,1024]{1,0:T(4,128)}, u32[]{:S(2)}) copy-start(f32[3,1024]{1,0:T(4,128)} %param.12) | copy-start | bytes 36868
  154.8 5.8 %copy-start.3 = (f32[3,1024]{1,0:T(4,128)S(1)}, f32[3,1024]{1,0:T(4,128)}, u32[]{:S(2)}) copy-start(f32[3,1024]{1,0:T(4,128)} %param.13) | copy-start | bytes 36868
  154.8 24.9 %copy-start = (bf16[3,4,256,256]{3,2,1,0:T(8,128)(2,1)S(1)}, bf16[3,4,256,256]{3,2,1,0:T(8,128)(2,1)}, u32[]{:S(2)}) copy-start(bf16[3,4,256,256]{3,2,1,0:T(8,128)(2,1)} %param.9) | copy-start | bytes 4718596
  159.9 120.5 %all-gather.10.cloned.1.call-start = ((), (), s32[]{:S(2)}) async-start(), calls=%async_computation.6 | async-start | bytes 7077888 | tf_op jit(solution)/shard_map/all_gather | solution.py:38
  160.5 164.1 %reduce-scatter.6.cloned.1.call-start = ((), (), s32[]{:S(2)}) async-start(), calls=%async_computation.7 | async-start | bytes 1966080 | tf_op jit(solution)/shard_map/reduce_scatter | solution.py:44
  297.9 63.2 %all-gather.12.cloned.1.call-start = ((), (), s32[]{:S(2)}) async-start(), calls=%async_computation.8 | async-start | bytes 1966080 | tf_op jit(solution)/shard_map/all_gather | solution.py:72
  325.6 5.3 %collective-permute-start.2 = (bf16[256,8]{1,0:T(8,128)(2,1)S(1)}, bf16[256,8]{1,0:T(8,128)(2,1)S(1)}, u32[]{:S(2)}, u32[]{:S(2)}) collective-permute-start(bf16[256,8]{1,0:T(8,128)(2,1)S(1)} %get-tuple-element.22), channel_id=1, source_target_pairs={{0,4},{4,8},{8,12},{12,16},{16,20},{20,24},{24,28},{1,5},{5,9},{9,... | collective-permute-start | bytes 12296 | tf_op jit(solution)/shard_map/ppermute | solution.py:17
  328.9 6.2 %collective-permute-start.3 = (bf16[256,8]{1,0:T(8,128)(2,1)S(1)}, bf16[256,8]{1,0:T(8,128)(2,1)S(1)}, u32[]{:S(2)}, u32[]{:S(2)}) collective-permute-start(bf16[256,8]{1,0:T(8,128)(2,1)S(1)} %get-tuple-element.23), channel_id=1, source_target_pairs={{4,0},{8,4},{12,8},{16,12},{20,16},{24,20},{28,24},{5,1},{9,5},{13... | collective-permute-start | bytes 12296 | tf_op jit(solution)/shard_map/ppermute | solution.py:18
  341.3 69.2 %reduce-scatter.8.cloned.1.call-start = ((), (), s32[]{:S(2)}) async-start(), calls=%async_computation.9 | async-start | bytes 1966080 | tf_op jit(solution)/shard_map/reduce_scatter | solution.py:44
  361.1 2.4 copy-start.4
  381.2 65.8 %all-gather.14.cloned.1.call-start = ((), (), s32[]{:S(2)}) async-start(), calls=%async_computation.10 | async-start | bytes 1966080 | tf_op jit(solution)/shard_map/all_gather | solution.py:72
  411.5 5.3 %collective-permute-start.4 = (bf16[256,8]{1,0:T(8,128)(2,1)S(1)}, bf16[256,8]{1,0:T(8,128)(2,1)S(1)}, u32[]{:S(2)}, u32[]{:S(2)}) collective-permute-start(bf16[256,8]{1,0:T(8,128)(2,1)S(1)} %get-tuple-element.20), channel_id=1, source_target_pairs={{0,4},{4,8},{8,12},{12,16},{16,20},{20,24},{24,28},{1,5},{5,9},{9,... | collective-permute-start | bytes 12296 | tf_op jit(solution)/shard_map/ppermute | solution.py:17
  414.8 6.2 %collective-permute-start.5 = (bf16[256,8]{1,0:T(8,128)(2,1)S(1)}, bf16[256,8]{1,0:T(8,128)(2,1)S(1)}, u32[]{:S(2)}, u32[]{:S(2)}) collective-permute-start(bf16[256,8]{1,0:T(8,128)(2,1)S(1)} %get-tuple-element.21), channel_id=1, source_target_pairs={{4,0},{8,4},{12,8},{16,12},{20,16},{24,20},{28,24},{5,1},{9,5},{13... | collective-permute-start | bytes 12296 | tf_op jit(solution)/shard_map/ppermute | solution.py:18
  447.0 2.4 copy-start.5
Sparse Core Ops, SparseCore 0:
  9.4 102.1 all-gather.5
  116.8 26.2 reduce-scatter.3
  160.1 19.5 all-gather.7
  181.7 98.6 all-gather.9
  298.0 26.4 reduce-scatter.5
  341.4 19.6 all-gather.11
  381.3 29.1 reduce-scatter.7
  427.3 19.6 all-gather.13
where the time goes:
time: 469 us; the launch traced here: 468 us
  waiting for transfers between devices  359 us (77%)
  matrix products  39.2 us (8%)
  other arithmetic  20.4 us (4%)
  blocking collectives  17.7 us (4%)
  starting transfers between devices  14.5 us (3%)
  between operations  13.8 us (3%)
    all_gather x1, waiting for transfers between devices, on_device(): lax.all_gather(in_proj, 'sp', axis=2, tiled=True)  104 us
    all_gather x1, waiting for transfers between devices, on_device(): lax.all_gather(out_proj, 'sp', axis=1, tiled=True)  98.7 us
    reduce_scatter x3, waiting for transfers between devices, on_device(): lax.psum_scatter(lax.dot_general(in_block, stream, (((0,), (1,)), ((), ()...  82.1 us
    all_gather x3, waiting for transfers between devices, on_device(): all_differ = lax.all_gather(differ, 'tp', axis=0, tiled=True)  58.3 us
    psum x3, blocking collectives, on_device(): lax.psum((jnp.sum(resid, axis=1), jnp.sum(resid * resid, axis=1)), 'tp')  17.7 us
    dot_general x3, matrix products, on_device(): lax.dot_general(in_block, stream, (((0,), (1,)), ((), ())), preferred_ele...  16.8 us
    dot_general x3, matrix products, on_device(): lax.dot_general(mixed_all, out_block, (((0,), (0,)), ((), ())), preferred...  16 us
    convert_element_type x3, other arithmetic, on_device(): differ = (pooled - projected.astype(jnp.float32)).astype(jnp.bfloat16)  15 us
  transfers between devices with their start and end apart: 14, of which 14 were waited for; matrix products, arithmetic and copies ran while one was open for 0% of the time, Pallas kernels for 0%

commit v1 on v0

--- a/solution.py
+++ b/solution.py
@@ -5,6 +5,22 @@
 
 pool_windows = (2, 4, 8, 16)
 norm_eps = 1e-05
+
+
+def review_notes_over_axis(q_in, row_dim):
+    axis_len = lax.axis_size("tp")
+    heard = q_in
+    series = [heard]
+    spare = [(dev_i - 1, dev_i) for dev_i in range(1, axis_len)] + [(axis_len - 1, 0)]
+    for _ in [*range(axis_len - 1)]:
+        heard = lax.ppermute(heard, "tp", spare)
+        series += [heard]
+    placed = jnp.roll(
+        jnp.concatenate([*reversed(series)], axis=row_dim),
+        (lax.axis_index("tp") + 1) * heard.shape[row_dim],
+        axis=row_dim,
+    )
+    return placed
 
 
 def padded(array, sides, width):
@@ -69,7 +85,7 @@
                 own_rows, window_total / (high_edge - low_edge).astype(jnp.float32)[None, :], pooled
             )
         differ = (pooled - projected.astype(jnp.float32)).astype(jnp.bfloat16)
-        all_differ = lax.all_gather(differ, "tp", axis=0, tiled=True)
+        all_differ = review_notes_over_axis(differ, 0)
         grouped = all_differ.reshape(4, group_width, rows_dev)
         mixed_all = jnp.einsum(
             "gcd,gct->gdt", group_mix[layer_idx], grouped, preferred_element_type=jnp.float32

time: 469 us -> 456 us (0.972)
  waiting for transfers between devices: 359 us -> 316 us
  other arithmetic: 20.4 us -> 49.9 us
    ppermute x0 -> x9, waiting for transfers between devices: none -> 64.6 us  [review_notes_over_axis(): heard = lax.ppermute(heard, 'tp', spare)]
    all_gather x3 -> x0, waiting for transfers between devices: 58.3 us -> none  [on_device(): all_differ = lax.all_gather(differ, 'tp', axis=0, tiled=True)]
    all_gather x1, waiting for transfers between devices: 98.7 us -> 51.5 us  [on_device(): lax.all_gather(out_proj, 'sp', axis=1, tiled=True)]
    concatenate x0 -> x3, other arithmetic: none -> 31.6 us  [review_notes_over_axis(): jnp.roll(jnp.concatenate([*reversed(series)], axis=row_dim), (lax.axis_in...]
  transfers between devices with their start and end apart: 14 -> 20, of which waited for: 14 -> 20; matrix products, arithmetic and copies ran while one was open for 0% -> 4% of each run, Pallas kernels for 0% -> 0%
where the time goes in v1:
time: 456 us; the launch traced here: 451 us
  waiting for transfers between devices  316 us (69%)
  other arithmetic  49.9 us (11%)
  matrix products  34.8 us (8%)
  blocking collectives  18.2 us (4%)
  starting transfers between devices  15 us (3%)
  between operations  13.7 us (3%)
    all_gather x1, waiting for transfers between devices, on_device(): lax.all_gather(in_proj, 'sp', axis=2, tiled=True)  104 us
    reduce_scatter x3, waiting for transfers between devices, on_device(): lax.psum_scatter(lax.dot_general(in_block, stream, (((0,), (1,)), ((), ()...  80.2 us
    ppermute x9, waiting for transfers between devices, review_notes_over_axis(): heard = lax.ppermute(heard, 'tp', spare)  64.6 us
    all_gather x1, waiting for transfers between devices, on_device(): lax.all_gather(out_proj, 'sp', axis=1, tiled=True)  51.5 us
    concatenate x3, other arithmetic, review_notes_over_axis(): jnp.roll(jnp.concatenate([*reversed(series)], axis=row_dim), (lax.axis_in...  31.6 us
    psum x3, blocking collectives, on_device(): lax.psum((jnp.sum(resid, axis=1), jnp.sum(resid * resid, axis=1)), 'tp')  18.2 us
    dot_general x3, matrix products, on_device(): lax.dot_general(in_block, stream, (((0,), (1,)), ((), ())), preferred_ele...  16.8 us
    dot_general x3, matrix products, on_device(): lax.dot_general(mixed_all, out_block, (((0,), (0,)), ((), ())), preferred...  16 us
  transfers between devices with their start and end apart: 20, of which 20 were waited for; matrix products, arithmetic and copies ran while one was open for 4% of the time, Pallas kernels for 0%

profile of v1, /device:TPU:0, one launch (start us, length us, event | category | flops | bytes accessed | tf_op | source)
XLA Modules:
  0.0 451.1 jit_solution(18260733876675316424)
XLA Ops:
  6.5 0.7 all-gather.3.cloned.1.call-update
  7.3 104.3 %all-gather.3.cloned.1.call-done = bf16[3,1024,1024]{2,1,0:T(8,128)(2,1)} async-done(((bf16[3,1024,128]{2,1,0:T(8,128)(2,1)}), bf16[3,1024,1024]{2,1,0:T(8,128)(2,1)}) %all-gather.3.cloned.1.call-update) | async-done | bytes 6291472 | tf_op jit(solution)/shard_map/all_gather | solution.py:53
  111.6 5.0 %fusion.6 = bf16[1024,768]{1,0:T(8,128)(2,1)} fusion(bf16[768,1024]{1,0:T(8,128)(2,1)} %param.9, bf16[3,1024,1024]{2,1,0:T(8,128)(2,1)} %all-gather.3.cloned.1.call-done), kind=kOutput, calls=%fused_computation.48 | convolution fusion | flops 1611399168 | bytes 5242880 | tf_op jit(solution)/shard_map/dot_general | solution.py:61
  116.7 0.7 all-gather.5.cloned.1.call-update
  117.5 25.5 %reduce-scatter.4.cloned.1.call-done = bf16[256,768]{1,0:T(8,128)(2,1)} async-done(((bf16[1024,768]{1,0:T(8,128)(2,1)}), bf16[256,768]{1,0:T(8,128)(2,1)}) %reduce-scatter.4.cloned.1.call-update) | async-done | bytes 393232 | tf_op jit(solution)/shard_map/reduce_scatter | solution.py:60
  143.1 1.0 fusion.79
  144.0 3.4 collective-permute-start
  147.4 1.3 collective-permute-start.1
  149.3 4.3 collective-permute-done.1
  153.6 1.2 maximum_convert_fusion
  154.8 4.3 fusion.65
  159.2 7.2 %collective-permute-done.2 = bf16[256,768]{1,0:T(8,128)(2,1)S(1)} collective-permute-done((bf16[256,768]{1,0:T(8,128)(2,1)S(1)}, bf16[256,768]{1,0:T(8,128)(2,1)S(1)}, u32[]{:S(2)}, u32[]{:S(2)}) %collective-permute-start.2) | collective-permute-done | bytes 393248 | tf_op jit(solution)/shard_map/ppermute | solution.py:16
  166.5 7.1 %collective-permute-done.3 = bf16[256,768]{1,0:T(8,128)(2,1)S(1)} collective-permute-done((bf16[256,768]{1,0:T(8,128)(2,1)S(1)}, bf16[256,768]{1,0:T(8,128)(2,1)S(1)}, u32[]{:S(2)}, u32[]{:S(2)}) %collective-permute-start.3) | collective-permute-done | bytes 393248 | tf_op jit(solution)/shard_map/ppermute | solution.py:16
  174.1 7.1 %collective-permute-done.4 = bf16[256,768]{1,0:T(8,128)(2,1)S(1)} collective-permute-done((bf16[256,768]{1,0:T(8,128)(2,1)S(1)}, bf16[256,768]{1,0:T(8,128)(2,1)S(1)}, u32[]{:S(2)}, u32[]{:S(2)}) %collective-permute-start.4) | collective-permute-done | bytes 393248 | tf_op jit(solution)/shard_map/ppermute | solution.py:16
  181.3 10.5 %fusion.26 = bf16[1024,768]{1,0:T(8,128)(2,1)S(1)} fusion(s32[]{:T(128)S(6)} %select_n.83, bf16[256,768]{1,0:T(8,128)(2,1)S(1)} %collective-permute-done.4, bf16[256,768]{1,0:T(8,128)(2,1)S(1)} %collective-permute-done.3, bf16[256,768]{1,0:T(8,128)(2,1)S(1)} %collective-permute-done.2, bf16[256,768]{1,0:T(8,128)(2,1)S(1)} %fusion.65), kind=kLoop, calls=%fused_computation.68 | loop fusion | flops 12582912 | bytes 3145732 | tf_op jit(solution)/shard_map/jit(_roll_dynamic)/concatenate | solution.py:18
  192.5 51.5 %all-gather.5.cloned.1.call-done = bf16[3,1024,1024]{2,1,0:T(8,128)(2,1)} async-done(((bf16[3,128,1024]{2,1,0:T(8,128)(2,1)}), bf16[3,1024,1024]{2,1,0:T(8,128)(2,1)}) %all-gather.5.cloned.1.call-update) | async-done | bytes 6291472 | tf_op jit(solution)/shard_map/all_gather | solution.py:54
  244.0 5.8 %fusion.76 = (f32[768]{0:T(1024)S(1)}, f32[768]{0:T(1024)S(1)}, f32[768,1024]{1,0:T(8,128)}) fusion(bf16[1024,768]{1,0:T(8,128)(2,1)S(1)} %bitcast.86, bf16[3,1024,1024]{2,1,0:T(8,128)(2,1)} %all-gather.5.cloned.1.call-done, bf16[768,1024]{1,0:T(8,128)(2,1)} %param.9), kind=kOutput, calls=%fused_computation.164 | convolution fusion | flops 1615329792 | bytes 8394752 | tf_op jit(solution)/shard_map/dot_general | solution.py:94
  249.8 5.7 %all-reduce.2 = (f32[768]{0:T(1024)S(1)}, f32[768]{0:T(1024)S(1)}) all-reduce(f32[768]{0:T(1024)S(1)} %get-tuple-element.11, f32[768]{0:T(1024)S(1)} %get-tuple-element.10), channel_id=1, replica_groups=mesh['sp'=8,'tp'=4] {'tp'}, use_global_device_ids=true, to_apply=%region_4.6 | all-reduce | flops 1536 | bytes 12288 | tf_op jit(solution)/shard_map/psum | solution.py:98
  255.5 5.9 %fusion.31 = bf16[1024,768]{1,0:T(8,128)(2,1)} fusion(bf16[3,1024,1024]{2,1,0:T(8,128)(2,1)} %all-gather.3.cloned.1.call-done, f32[768,1024]{1,0:T(8,128)} %get-tuple-element.39, f32[1024]{0:T(1024)S(1)} %bitcast.95, f32[1024]{0:T(1024)S(1)} %bitcast.93, f32[768]{0:T(1024)S(1)} %get-tuple-element.38, f32[768]{0:T(1024)S(1)} %get-tuple-element.37), kind=kOutput, calls=%fused_computation.73 | convolution fusion | flops 1615331328 | bytes 6830080 | tf_op jit(solution)/shard_map/dot_general | solution.py:61
  261.5 26.6 %reduce-scatter.6.cloned.1.call-done = bf16[256,768]{1,0:T(8,128)(2,1)} async-done(((bf16[1024,768]{1,0:T(8,128)(2,1)}), bf16[256,768]{1,0:T(8,128)(2,1)}) %reduce-scatter.6.cloned.1.call-update) | async-done | bytes 393232 | tf_op jit(solution)/shard_map/reduce_scatter | solution.py:60
  288.0 1.0 fusion.78
  289.0 3.4 collective-permute-start.5
  292.4 1.5 collective-permute-start.6
  294.3 4.3 collective-permute-done.6
  298.6 1.2 maximum_convert_fusion.1
  299.8 4.3 fusion.66
  304.1 7.2 %collective-permute-done.7 = bf16[256,768]{1,0:T(8,128)(2,1)S(1)} collective-permute-done((bf16[256,768]{1,0:T(8,128)(2,1)S(1)}, bf16[256,768]{1,0:T(8,128)(2,1)S(1)}, u32[]{:S(2)}, u32[]{:S(2)}) %collective-permute-start.7) | collective-permute-done | bytes 393248 | tf_op jit(solution)/shard_map/ppermute | solution.py:16
  311.3 7.2 %collective-permute-done.8 = bf16[256,768]{1,0:T(8,128)(2,1)S(1)} collective-permute-done((bf16[256,768]{1,0:T(8,128)(2,1)S(1)}, bf16[256,768]{1,0:T(8,128)(2,1)S(1)}, u32[]{:S(2)}, u32[]{:S(2)}) %collective-permute-start.8) | collective-permute-done | bytes 393248 | tf_op jit(solution)/shard_map/ppermute | solution.py:16
  318.6 7.2 %collective-permute-done.9 = bf16[256,768]{1,0:T(8,128)(2,1)S(1)} collective-permute-done((bf16[256,768]{1,0:T(8,128)(2,1)S(1)}, bf16[256,768]{1,0:T(8,128)(2,1)S(1)}, u32[]{:S(2)}, u32[]{:S(2)}) %collective-permute-start.9) | collective-permute-done | bytes 393248 | tf_op jit(solution)/shard_map/ppermute | solution.py:16
  325.7 10.5 %fusion.19 = bf16[1024,768]{1,0:T(8,128)(2,1)S(1)} fusion(s32[]{:T(128)S(6)} %select_n.83, bf16[256,768]{1,0:T(8,128)(2,1)S(1)} %collective-permute-done.9, bf16[256,768]{1,0:T(8,128)(2,1)S(1)} %collective-permute-done.8, bf16[256,768]{1,0:T(8,128)(2,1)S(1)} %collective-permute-done.7, bf16[256,768]{1,0:T(8,128)(2,1)S(1)} %fusion.66), kind=kLoop, calls=%fused_computation.61 | loop fusion | flops 12582912 | bytes 3145732 | tf_op jit(solution)/shard_map/jit(_roll_dynamic)/concatenate | solution.py:18
  336.3 0.7 multiply_convert_fusion.1
  337.0 5.9 %fusion.75 = (f32[768]{0:T(1024)S(1)}, f32[768]{0:T(1024)S(1)}, f32[768,1024]{1,0:T(8,128)}) fusion(bf16[1024,768]{1,0:T(8,128)(2,1)S(1)} %bitcast.85, bf16[3,1024,1024]{2,1,0:T(8,128)(2,1)} %all-gather.5.cloned.1.call-done, f32[1024]{0:T(1024)S(1)} %bitcast.96, f32[1024]{0:T(1024)S(1)} %bitcast.94, f32[768]{0:T(1024)S(1)} %get-tuple-element.38, ...), kind=kOutput, calls=%fused_computation.163 | convolution fusion | flops 1619261952 | bytes 9981952 | tf_op jit(solution)/shard_map/dot_general | solution.py:94
  342.8 6.3 %all-reduce.1 = (f32[768]{0:T(1024)S(1)}, f32[768]{0:T(1024)S(1)}) all-reduce(f32[768]{0:T(1024)S(1)} %get-tuple-element.9, f32[768]{0:T(1024)S(1)} %get-tuple-element.8), channel_id=1, replica_groups=mesh['sp'=8,'tp'=4] {'tp'}, use_global_device_ids=true, to_apply=%region_9.11 | all-reduce | flops 1536 | bytes 12288 | tf_op jit(solution)/shard_map/psum | solution.py:98
  349.2 5.9 %fusion.30 = bf16[1024,768]{1,0:T(8,128)(2,1)} fusion(bf16[3,1024,1024]{2,1,0:T(8,128)(2,1)} %all-gather.3.cloned.1.call-done, f32[768,1024]{1,0:T(8,128)} %get-tuple-element.40, f32[1024]{0:T(1024)S(1)} %bitcast.91, f32[1024]{0:T(1024)S(1)} %bitcast.89, f32[768]{0:T(1024)S(1)} %get-tuple-element.36, f32[768]{0:T(1024)S(1)} %get-tuple-element.35), kind=kOutput, calls=%fused_computation.72 | convolution fusion | flops 1615331328 | bytes 6830080 | tf_op jit(solution)/shard_map/dot_general | solution.py:61
  355.1 28.1 %reduce-scatter.8.cloned.1.call-done = bf16[256,768]{1,0:T(8,128)(2,1)} async-done(((bf16[1024,768]{1,0:T(8,128)(2,1)}), bf16[256,768]{1,0:T(8,128)(2,1)}) %reduce-scatter.8.cloned.1.call-update) | async-done | bytes 393232 | tf_op jit(solution)/shard_map/reduce_scatter | solution.py:60
  383.2 1.0 fusion.77
  384.2 3.4 collective-permute-start.10
  387.6 1.3 collective-permute-start.11
  389.5 4.3 collective-permute-done.11
  393.7 1.2 maximum_convert_fusion.2
  395.0 4.3 fusion.67
  399.3 7.2 %collective-permute-done.12 = bf16[256,768]{1,0:T(8,128)(2,1)S(1)} collective-permute-done((bf16[256,768]{1,0:T(8,128)(2,1)S(1)}, bf16[256,768]{1,0:T(8,128)(2,1)S(1)}, u32[]{:S(2)}, u32[]{:S(2)}) %collective-permute-start.12) | collective-permute-done | bytes 393248 | tf_op jit(solution)/shard_map/ppermute | solution.py:16
  406.5 7.2 %collective-permute-done.13 = bf16[256,768]{1,0:T(8,128)(2,1)S(1)} collective-permute-done((bf16[256,768]{1,0:T(8,128)(2,1)S(1)}, bf16[256,768]{1,0:T(8,128)(2,1)S(1)}, u32[]{:S(2)}, u32[]{:S(2)}) %collective-permute-start.13) | collective-permute-done | bytes 393248 | tf_op jit(solution)/shard_map/ppermute | solution.py:16
  413.7 7.2 %collective-permute-done.14 = bf16[256,768]{1,0:T(8,128)(2,1)S(1)} collective-permute-done((bf16[256,768]{1,0:T(8,128)(2,1)S(1)}, bf16[256,768]{1,0:T(8,128)(2,1)S(1)}, u32[]{:S(2)}, u32[]{:S(2)}) %collective-permute-start.14) | collective-permute-done | bytes 393248 | tf_op jit(solution)/shard_map/ppermute | solution.py:16
  420.9 10.5 %fusion.12 = bf16[1024,768]{1,0:T(8,128)(2,1)S(1)} fusion(s32[]{:T(128)S(6)} %select_n.83, bf16[256,768]{1,0:T(8,128)(2,1)S(1)} %collective-permute-done.14, bf16[256,768]{1,0:T(8,128)(2,1)S(1)} %collective-permute-done.13, bf16[256,768]{1,0:T(8,128)(2,1)S(1)} %collective-permute-done.12, bf16[256,768]{1,0:T(8,128)(2,1)S(1)} %fusion.67), kind=kLoop, calls=%fused_computation.54 | loop fusion | flops 12582912 | bytes 3145732 | tf_op jit(solution)/shard_map/jit(_roll_dynamic)/concatenate | solution.py:18
  432.1 4.4 fusion.74
  436.5 6.1 %all-reduce = (f32[768]{0:T(1024)S(1)}, f32[768]{0:T(1024)S(1)}) all-reduce(f32[768]{0:T(1024)S(1)} %get-tuple-element.7, f32[768]{0:T(1024)S(1)} %get-tuple-element.6), channel_id=1, replica_groups=mesh['sp'=8,'tp'=4] {'tp'}, use_global_device_ids=true, to_apply=%region_14.16 | all-reduce | flops 1536 | bytes 12288 | tf_op jit(solution)/shard_map/psum | solution.py:98
  442.6 1.7 add_convert_fusion
  (47 shorter events, 3.9 us)
Async XLA Ops:
  6.5 105.1 %all-gather.3.cloned.1.call-start = ((), (), s32[]{:S(2)}) async-start(), calls=%async_computation.3 | async-start | bytes 7077888 | tf_op jit(solution)/shard_map/all_gather | solution.py:53
  7.3 135.8 %reduce-scatter.4.cloned.1.call-start = ((), (), s32[]{:S(2)}) async-start(), calls=%async_computation.4 | async-start | bytes 1966080 | tf_op jit(solution)/shard_map/reduce_scatter | solution.py:60
  116.7 127.3 %all-gather.5.cloned.1.call-start = ((), (), s32[]{:S(2)}) async-start(), calls=%async_computation.5 | async-start | bytes 7077888 | tf_op jit(solution)/shard_map/all_gather | solution.py:54
  117.4 170.6 %reduce-scatter.6.cloned.1.call-start = ((), (), s32[]{:S(2)}) async-start(), calls=%async_computation.6 | async-start | bytes 1966080 | tf_op jit(solution)/shard_map/reduce_scatter | solution.py:60
  144.0 5.3 %collective-permute-start = (bf16[256,8]{1,0:T(8,128)(2,1)S(1)}, bf16[256,8]{1,0:T(8,128)(2,1)S(1)}, u32[]{:S(2)}, u32[]{:S(2)}) collective-permute-start(bf16[256,8]{1,0:T(8,128)(2,1)S(1)} %get-tuple-element.25), channel_id=1, source_target_pairs={{0,4},{4,8},{8,12},{12,16},{16,20},{20,24},{24,28},{1,5},{5,9},{9,... | collective-permute-start | bytes 12296 | tf_op jit(solution)/shard_map/ppermute | solution.py:33
  147.4 6.2 %collective-permute-start.1 = (bf16[256,8]{1,0:T(8,128)(2,1)S(1)}, bf16[256,8]{1,0:T(8,128)(2,1)S(1)}, u32[]{:S(2)}, u32[]{:S(2)}) collective-permute-start(bf16[256,8]{1,0:T(8,128)(2,1)S(1)} %get-tuple-element.26), channel_id=1, source_target_pairs={{4,0},{8,4},{12,8},{16,12},{20,16},{24,20},{28,24},{5,1},{9,5},{13... | collective-permute-start | bytes 12296 | tf_op jit(solution)/shard_map/ppermute | solution.py:34
  154.8 11.6 %copy-start.1 = (f32[3,1024]{1,0:T(4,128)S(1)}, f32[3,1024]{1,0:T(4,128)}, u32[]{:S(2)}) copy-start(f32[3,1024]{1,0:T(4,128)} %param.12) | copy-start | bytes 36868
  154.8 19.3 %copy-start.2 = (f32[3,1024]{1,0:T(4,128)S(1)}, f32[3,1024]{1,0:T(4,128)}, u32[]{:S(2)}) copy-start(f32[3,1024]{1,0:T(4,128)} %param.14) | copy-start | bytes 36868
  154.8 19.3 %copy-start.3 = (f32[3,1024]{1,0:T(4,128)S(1)}, f32[3,1024]{1,0:T(4,128)}, u32[]{:S(2)}) copy-start(f32[3,1024]{1,0:T(4,128)} %param.15) | copy-start | bytes 36868
  159.1 32.7 %copy-start = (bf16[3,4,256,256]{3,2,1,0:T(8,128)(2,1)S(1)}, bf16[3,4,256,256]{3,2,1,0:T(8,128)(2,1)}, u32[]{:S(2)}) copy-start(bf16[3,4,256,256]{3,2,1,0:T(8,128)(2,1)} %param.11) | copy-start | bytes 4718596
  159.2 7.3 %collective-permute-start.2 = (bf16[256,768]{1,0:T(8,128)(2,1)S(1)}, bf16[256,768]{1,0:T(8,128)(2,1)S(1)}, u32[]{:S(2)}, u32[]{:S(2)}) collective-permute-start(bf16[256,768]{1,0:T(8,128)(2,1)S(1)} %fusion.65), channel_id=1, source_target_pairs={{0,1},{1,2},{2,3},{3,0},{4,5},{5,6},{6,7},{7,4},{8,9},{9,10},{10,1... | collective-permute-start | bytes 1179656 | tf_op jit(solution)/shard_map/ppermute | solution.py:16
  166.4 7.2 %collective-permute-start.3 = (bf16[256,768]{1,0:T(8,128)(2,1)S(1)}, bf16[256,768]{1,0:T(8,128)(2,1)S(1)}, u32[]{:S(2)}, u32[]{:S(2)}) collective-permute-start(bf16[256,768]{1,0:T(8,128)(2,1)S(1)} %collective-permute-done.2), channel_id=1, source_target_pairs={{0,1},{1,2},{2,3},{3,0},{4,5},{5,6},{6,7},{7,4},{8,9},{9,10},{10,1... | collective-permute-start | bytes 1179656 | tf_op jit(solution)/shard_map/ppermute | solution.py:16
  173.6 7.6 %collective-permute-start.4 = (bf16[256,768]{1,0:T(8,128)(2,1)S(1)}, bf16[256,768]{1,0:T(8,128)(2,1)S(1)}, u32[]{:S(2)}, u32[]{:S(2)}) collective-permute-start(bf16[256,768]{1,0:T(8,128)(2,1)S(1)} %collective-permute-done.3), channel_id=1, source_target_pairs={{0,1},{1,2},{2,3},{3,0},{4,5},{5,6},{6,7},{7,4},{8,9},{9,10},{10,1... | collective-permute-start | bytes 1179656 | tf_op jit(solution)/shard_map/ppermute | solution.py:16
  261.4 121.8 %reduce-scatter.8.cloned.1.call-start = ((), (), s32[]{:S(2)}) async-start(), calls=%async_computation.7 | async-start | bytes 1966080 | tf_op jit(solution)/shard_map/reduce_scatter | solution.py:60
  289.0 5.3 %collective-permute-start.5 = (bf16[256,8]{1,0:T(8,128)(2,1)S(1)}, bf16[256,8]{1,0:T(8,128)(2,1)S(1)}, u32[]{:S(2)}, u32[]{:S(2)}) collective-permute-start(bf16[256,8]{1,0:T(8,128)(2,1)S(1)} %get-tuple-element.23), channel_id=1, source_target_pairs={{0,4},{4,8},{8,12},{12,16},{16,20},{20,24},{24,28},{1,5},{5,9},{9,... | collective-permute-start | bytes 12296 | tf_op jit(solution)/shard_map/ppermute | solution.py:33
  292.4 6.2 %collective-permute-start.6 = (bf16[256,8]{1,0:T(8,128)(2,1)S(1)}, bf16[256,8]{1,0:T(8,128)(2,1)S(1)}, u32[]{:S(2)}, u32[]{:S(2)}) collective-permute-start(bf16[256,8]{1,0:T(8,128)(2,1)S(1)} %get-tuple-element.24), channel_id=1, source_target_pairs={{4,0},{8,4},{12,8},{16,12},{20,16},{24,20},{28,24},{5,1},{9,5},{13... | collective-permute-start | bytes 12296 | tf_op jit(solution)/shard_map/ppermute | solution.py:34
  304.1 7.3 %collective-permute-start.7 = (bf16[256,768]{1,0:T(8,128)(2,1)S(1)}, bf16[256,768]{1,0:T(8,128)(2,1)S(1)}, u32[]{:S(2)}, u32[]{:S(2)}) collective-permute-start(bf16[256,768]{1,0:T(8,128)(2,1)S(1)} %fusion.66), channel_id=1, source_target_pairs={{0,1},{1,2},{2,3},{3,0},{4,5},{5,6},{6,7},{7,4},{8,9},{9,10},{10,1... | collective-permute-start | bytes 1179656 | tf_op jit(solution)/shard_map/ppermute | solution.py:16
  311.3 7.2 %collective-permute-start.8 = (bf16[256,768]{1,0:T(8,128)(2,1)S(1)}, bf16[256,768]{1,0:T(8,128)(2,1)S(1)}, u32[]{:S(2)}, u32[]{:S(2)}) collective-permute-start(bf16[256,768]{1,0:T(8,128)(2,1)S(1)} %collective-permute-done.7), channel_id=1, source_target_pairs={{0,1},{1,2},{2,3},{3,0},{4,5},{5,6},{6,7},{7,4},{8,9},{9,10},{10,1... | collective-permute-start | bytes 1179656 | tf_op jit(solution)/shard_map/ppermute | solution.py:16
  318.5 7.2 %collective-permute-start.9 = (bf16[256,768]{1,0:T(8,128)(2,1)S(1)}, bf16[256,768]{1,0:T(8,128)(2,1)S(1)}, u32[]{:S(2)}, u32[]{:S(2)}) collective-permute-start(bf16[256,768]{1,0:T(8,128)(2,1)S(1)} %collective-permute-done.8), channel_id=1, source_target_pairs={{0,1},{1,2},{2,3},{3,0},{4,5},{5,6},{6,7},{7,4},{8,9},{9,10},{10,1... | collective-permute-start | bytes 1179656 | tf_op jit(solution)/shard_map/ppermute | solution.py:16
  318.5 18.4 %copy-start.4 = (f32[768,1024]{1,0:T(8,128)S(1)}, f32[768,1024]{1,0:T(8,128)}, u32[]{:S(2)}) copy-start(f32[768,1024]{1,0:T(8,128)} %get-tuple-element.39) | copy-start | bytes 9437188
  384.2 5.3 %collective-permute-start.10 = (bf16[256,8]{1,0:T(8,128)(2,1)S(1)}, bf16[256,8]{1,0:T(8,128)(2,1)S(1)}, u32[]{:S(2)}, u32[]{:S(2)}) collective-permute-start(bf16[256,8]{1,0:T(8,128)(2,1)S(1)} %get-tuple-element.21), channel_id=1, source_target_pairs={{0,4},{4,8},{8,12},{12,16},{16,20},{20,24},{24,28},{1,5},{5,9},{9,... | collective-permute-start | bytes 12296 | tf_op jit(solution)/shard_map/ppermute | solution.py:33
  387.6 6.2 %collective-permute-start.11 = (bf16[256,8]{1,0:T(8,128)(2,1)S(1)}, bf16[256,8]{1,0:T(8,128)(2,1)S(1)}, u32[]{:S(2)}, u32[]{:S(2)}) collective-permute-start(bf16[256,8]{1,0:T(8,128)(2,1)S(1)} %get-tuple-element.22), channel_id=1, source_target_pairs={{4,0},{8,4},{12,8},{16,12},{20,16},{24,20},{28,24},{5,1},{9,5},{13... | collective-permute-start | bytes 12296 | tf_op jit(solution)/shard_map/ppermute | solution.py:34
  399.3 7.3 %collective-permute-start.12 = (bf16[256,768]{1,0:T(8,128)(2,1)S(1)}, bf16[256,768]{1,0:T(8,128)(2,1)S(1)}, u32[]{:S(2)}, u32[]{:S(2)}) collective-permute-start(bf16[256,768]{1,0:T(8,128)(2,1)S(1)} %fusion.67), channel_id=1, source_target_pairs={{0,1},{1,2},{2,3},{3,0},{4,5},{5,6},{6,7},{7,4},{8,9},{9,10},{10,1... | collective-permute-start | bytes 1179656 | tf_op jit(solution)/shard_map/ppermute | solution.py:16
  406.5 7.2 %collective-permute-start.13 = (bf16[256,768]{1,0:T(8,128)(2,1)S(1)}, bf16[256,768]{1,0:T(8,128)(2,1)S(1)}, u32[]{:S(2)}, u32[]{:S(2)}) collective-permute-start(bf16[256,768]{1,0:T(8,128)(2,1)S(1)} %collective-permute-done.12), channel_id=1, source_target_pairs={{0,1},{1,2},{2,3},{3,0},{4,5},{5,6},{6,7},{7,4},{8,9},{9,10},{10,1... | collective-permute-start | bytes 1179656 | tf_op jit(solution)/shard_map/ppermute | solution.py:16
  413.7 7.2 %collective-permute-start.14 = (bf16[256,768]{1,0:T(8,128)(2,1)S(1)}, bf16[256,768]{1,0:T(8,128)(2,1)S(1)}, u32[]{:S(2)}, u32[]{:S(2)}) collective-permute-start(bf16[256,768]{1,0:T(8,128)(2,1)S(1)} %collective-permute-done.13), channel_id=1, source_target_pairs={{0,1},{1,2},{2,3},{3,0},{4,5},{5,6},{6,7},{7,4},{8,9},{9,10},{10,1... | collective-permute-start | bytes 1179656 | tf_op jit(solution)/shard_map/ppermute | solution.py:16
  413.7 18.4 %copy-start.5 = (f32[768,1024]{1,0:T(8,128)S(1)}, f32[768,1024]{1,0:T(8,128)}, u32[]{:S(2)}) copy-start(f32[768,1024]{1,0:T(8,128)} %get-tuple-element.40) | copy-start | bytes 9437188
Sparse Core Ops, SparseCore 0:
  9.4 102.1 all-gather.2
  116.8 26.2 reduce-scatter.3
  145.2 98.6 all-gather.4
  261.6 26.4 reduce-scatter.5
  355.2 27.9 reduce-scatter.7
